TPU v7x, 32 devices: a whole 2x2x4 slice. The times are simulated.
32 devices in a mesh: ep: 4 (over y, x), tp: 8 (over z, core).
Axes of the slice: x: 2, y: 2, z: 4, core: 2. Of those that a mesh axis runs over, the one named last changes fastest.
Arguments:
- query_latent: bfloat16 [2048, 1024], P('ep'), may hold values from -6 to 6
- joint_latent: bfloat16 [2048, 512], P('ep'), may hold values from -6 to 6
- rotary_key: bfloat16 [2048, 32], P('ep'), may hold values from -60 to 60
- query_gain: float32 [1024], replicated, may hold values from 0.1 to 1.9
- joint_gain: float32 [512], replicated, may hold values from 0.1 to 1.9
- query_weight: bfloat16 [1024, 2048], P(None, 'tp'), may hold values from -0.1875 to 0.1875
- query_rotary: bfloat16 [1024, 1024], P(None, 'tp'), may hold values from -0.1875 to 0.1875
- key_weight: bfloat16 [512, 2048], P(None, 'tp'), may hold values from -0.25 to 0.25
- value_weight: bfloat16 [512, 2048], P(None, 'tp'), may hold values from -0.25 to 0.25
- output_weight: bfloat16 [2048, 2048], P('tp'), may hold values from -6 to 6
- expert_input: bfloat16 [2048, 2048], P('ep'), may hold values from -6 to 6
- expert_gain: float32 [2048], replicated, may hold values from 0.1 to 1.9
- routes: int32 [2048, 2], P('ep'), may hold values from 0 to 7, all different within a row; in each aligned block of 512 rows (0 to 511, 512 to 1023, ...) at most 192 rows name the same one
- route_weight: float32 [2048, 2], P('ep'), may hold values from 0.2 to 1
- gate_weight: bfloat16 [8, 2048, 4096], P('ep', None, 'tp'), may hold values from -0.125 to 0.125
- up_weight: bfloat16 [8, 2048, 4096], P('ep', None, 'tp'), may hold values from -0.125 to 0.125
- down_weight: bfloat16 [8, 4096, 2048], P('ep', 'tp'), may hold values from -0.09375 to 0.09375
Outputs:
- mixer_out: bfloat16 [2048, 2048], P(('ep', 'tp'))
- expert_out: bfloat16 [2048, 2048], P('ep', 'tp')
Inputs may be any that keep to these rules, and one draw needn't show every extreme that they name: `routes`: A row names 2 different experts. Among the rows of one device (aligned blocks of 512 rows) no expert is named by more than 192 rows, a bound that some block reaches.
All inputs are finite; a program needn't handle non-finite values.
Results may differ from a plain program's by a relative error of at most 0.019.
The roundings to bfloat16 on the way count: a program that leaves them out, or rounds other values in their place, can miss the bound.
Values may be sent and summed in bfloat16 or wider, within the bound.
A program may use at most 128 MiB of HBM per device.

v0:
```python
import functools

import jax
import jax.numpy as jnp
from jax import lax
from jax.experimental import pallas as pl
from jax.experimental.pallas import tpu as pltpu
from jax.sharding import PartitionSpec as P

NOPE = 64
VDIM = 64

NORM_EPSILON = 1e-06
ROTARY_BASE = 10000.0
F32 = jnp.float32
BF16 = jnp.bfloat16


def norm_rows(source, gain_vector):
    as_float = source.astype(F32)
    factor = lax.rsqrt(jnp.mean(as_float * as_float, axis=-1, keepdims=True) + NORM_EPSILON)
    return (as_float * factor * gain_vector).astype(BF16)


def rotation_tables(positions, width, copies):
    half_width = width // 2
    lane = jnp.arange(width * copies, dtype=jnp.int32) % width
    frequencies = ROTARY_BASE ** (-(lane % half_width).astype(F32) / half_width)
    angles = positions[:, None] * frequencies[None, :]
    sign = jnp.where(lane < half_width, -1.0, 1.0).astype(F32)
    return jnp.cos(angles), jnp.sin(angles) * sign[None, :]


def swap_matrix(width, copies):
    half_width = width // 2
    lane = jnp.arange(width * copies, dtype=jnp.int32)
    partner = (lane // width) * width + (lane % width + half_width) % width
    return (lane[:, None] == partner[None, :]).astype(BF16)


def attention_kernel(head_count, turn_width, scale, q_ref, qt_ref, kt_ref, tk_ref, v_ref, out_ref):
    turned_keys = tk_ref[...]
    pieces = []
    per_pair = 128 // VDIM
    for head in range(head_count):
        query = jnp.concatenate(
            [
                q_ref[:, head * NOPE : (head + 1) * NOPE],
                qt_ref[:, head * turn_width : (head + 1) * turn_width],
            ],
            axis=1,
        )
        keys = jnp.concatenate([kt_ref[head * NOPE : (head + 1) * NOPE, :], turned_keys], axis=0)
        scores = jnp.dot(query, keys, preferred_element_type=F32) * scale
        top = jnp.max(scores, axis=-1, keepdims=True)
        expo = jnp.exp(scores - top)
        total = jnp.sum(expo, axis=-1, keepdims=True)
        pair = head // per_pair
        mixed = jnp.dot(
            expo.astype(BF16), v_ref[:, pair * 128 : (pair + 1) * 128], preferred_element_type=F32
        )
        inner = head % per_pair
        mixed = mixed[:, inner * VDIM : (inner + 1) * VDIM]
        pieces.append((mixed / total).astype(BF16))
    out_ref[...] = jnp.concatenate(pieces, axis=1)


def attention(query_plain, query_turned, keys_t, turned_t, values, turn_width):
    rows, width = query_plain.shape
    tokens = values.shape[0]
    head_count = width // NOPE
    block = 128
    scale = (NOPE + turn_width) ** (-0.5)
    whole = lambda i: (0, 0)
    return pl.pallas_call(
        functools.partial(attention_kernel, head_count, turn_width, scale),
        grid=(rows // block,),
        in_specs=[
            pl.BlockSpec((block, width), lambda i: (i, 0)),
            pl.BlockSpec((block, query_turned.shape[1]), lambda i: (i, 0)),
            pl.BlockSpec(keys_t.shape, whole),
            pl.BlockSpec(turned_t.shape, whole),
            pl.BlockSpec(values.shape, whole),
        ],
        out_specs=pl.BlockSpec((block, head_count * VDIM), lambda i: (i, 0)),
        out_shape=jax.ShapeDtypeStruct((rows, head_count * VDIM), BF16),
        compiler_params=pltpu.CompilerParams(vmem_limit_bytes=40 * 1024 * 1024),
        cost_estimate=pl.CostEstimate(
            flops=40 * rows * tokens * head_count * (NOPE + turn_width),
            bytes_accessed=4 * tokens * width,
            transcendentals=rows * tokens * head_count,
        ),
        name="attention",
    )(query_plain, query_turned, keys_t, turned_t, values)


def half_of(source, parity, axis):
    half = source.shape[axis] // 2
    return lax.dynamic_slice_in_dim(source, parity * half, half, axis)


def swap_cores(source):
    size = lax.axis_size("tp")
    return lax.ppermute(source, "tp", [(i, i ^ 1) for i in range(size)])


def latent_part(joint_latent, rotary_key, joint_gain, parity):
    row_count = joint_latent.shape[0]
    turn_width = rotary_key.shape[1]
    positions = (lax.axis_index("ep") * row_count + jnp.arange(row_count, dtype=jnp.int32)).astype(F32)
    normed = half_of(norm_rows(joint_latent, joint_gain), parity, 1)
    cosine, sine = rotation_tables(positions, turn_width, 1)
    swapped = jnp.dot(rotary_key, swap_matrix(turn_width, 1), preferred_element_type=F32)
    turned = (rotary_key.astype(F32) * cosine + swapped * sine).astype(BF16)
    return jnp.concatenate([normed, turned], axis=1)


def token_mixer(
    latent,
    query_latent,
    query_gain,
    query_weight,
    query_rotary,
    key_weight,
    value_weight,
    turn_width,
    parity,
):
    mine, other, turned = latent
    row_count = query_latent.shape[0]
    positions = (lax.axis_index("ep") * row_count + jnp.arange(row_count, dtype=jnp.int32)).astype(F32)
    head_count = key_weight.shape[1] // NOPE
    query_normed = norm_rows(query_latent, query_gain)
    query_plain = jnp.dot(query_normed, query_weight, preferred_element_type=F32).astype(BF16)
    cosine, sine = rotation_tables(positions, turn_width, head_count)
    rotary_swapped = jnp.dot(
        query_rotary, swap_matrix(turn_width, head_count), preferred_element_type=F32
    ).astype(BF16)
    query_turned = (
        jnp.dot(query_normed, query_rotary, preferred_element_type=F32) * cosine
        + jnp.dot(query_normed, rotary_swapped, preferred_element_type=F32) * sine
    ).astype(BF16)

    normed = jnp.where(
        parity == 0,
        jnp.concatenate([mine, other], axis=1),
        jnp.concatenate([other, mine], axis=1),
    )
    keys_t = jnp.einsum("td,df->ft", normed, key_weight, preferred_element_type=F32).astype(BF16)
    values = jnp.dot(normed, value_weight, preferred_element_type=F32).astype(BF16)
    return attention(query_plain, query_turned, keys_t, turned.T, values, turn_width)


def column_blocks(weight, parity, blocks):
    width = weight.shape[2] // blocks
    return jnp.concatenate(
        [
            lax.dynamic_slice_in_dim(weight, (2 * z + parity) * width, width, 2)
            for z in range(blocks // 2)
        ],
        axis=2,
    )


def local(
    query_latent,
    joint_latent,
    rotary_key,
    query_gain,
    joint_gain,
    query_weight,
    query_rotary,
    key_weight,
    value_weight,
    output_weight,
    expert_input,
    expert_gain,
    routes,
    route_weight,
    gate_weight,
    up_weight,
    down_weight,
):
    parity = lax.axis_index("tp") % 2
    tp_size = lax.axis_size("tp")
    row_count, feature_width = expert_input.shape
    group_count = lax.axis_size("ep")
    local_count = gate_weight.shape[0]
    expert_count = local_count * group_count
    capacity = 3 * row_count // (2 * group_count)
    half = feature_width // 2

    part = latent_part(joint_latent, rotary_key, joint_gain, parity)
    part, expert_rows = lax.optimization_barrier((part, expert_input))
    gathered = lax.all_gather(part, "ep", axis=0, tiled=True)

    routes_t = routes.T
    names = jnp.arange(expert_count, dtype=jnp.int32)
    member = (routes_t[0][None, :] == names[:, None]) | (routes_t[1][None, :] == names[:, None])
    token = jnp.arange(row_count, dtype=jnp.int32)
    before = (token[:, None] < token[None, :]).astype(BF16)
    rank = jnp.dot(member.astype(BF16), before, preferred_element_type=F32).astype(jnp.int32)
    place = jnp.where(member, rank, -1)
    slots = jnp.arange(capacity, dtype=jnp.int32)
    chosen = (place[:, None, :] == slots[None, :, None]).astype(BF16)
    chosen = chosen.reshape(expert_count * capacity, row_count)
    rows_half = lax.optimization_barrier(half_of(norm_rows(expert_rows, expert_gain), parity, 1))
    outgoing = jnp.dot(chosen, rows_half, preferred_element_type=F32).astype(BF16)
    outgoing = outgoing.reshape(group_count, local_count, capacity, half)
    mine = lax.all_to_all(outgoing, "ep", split_axis=0, concat_axis=0, tiled=True)
    latent_half = gathered[:, : joint_latent.shape[1] // 2]
    attended = token_mixer(
        (latent_half, swap_cores(latent_half), gathered[:, joint_latent.shape[1] // 2 :]),
        query_latent,
        query_gain,
        query_weight,
        query_rotary,
        key_weight,
        value_weight,
        rotary_key.shape[1],
        parity,
    )
    mine, attended = lax.optimization_barrier((mine, attended))
    other = swap_cores(mine)
    mixer_out = lax.psum_scatter(
        jnp.dot(attended, output_weight, preferred_element_type=F32).astype(BF16),
        "tp",
        scatter_dimension=0,
        tiled=True,
    )

    def project(weight):
        return jnp.einsum(
            "secd,edf->secf", mine, half_of(weight, parity, 1), preferred_element_type=F32
        ) + jnp.einsum(
            "secd,edf->secf", other, half_of(weight, 1 - parity, 1), preferred_element_type=F32
        )

    gate_acts = project(gate_weight)
    up_acts = project(up_weight)
    hidden = (jax.nn.silu(gate_acts) * up_acts).astype(BF16)

    def down(side):
        return jnp.einsum(
            "secf,efd->secd",
            hidden,
            column_blocks(down_weight, side, tp_size),
            preferred_element_type=F32,
        ).astype(BF16)

    theirs = swap_cores(down(1 - parity))
    summed = (down(parity).astype(F32) + theirs.astype(F32)).astype(BF16)
    returned = lax.all_to_all(summed, "ep", split_axis=0, concat_axis=0, tiled=True)
    returned = returned.reshape(expert_count * capacity, half)

    def picked(k):
        slot = jnp.sum(
            jnp.where(routes_t[k][None, :] == names[:, None], names[:, None] * capacity + rank, 0),
            axis=0,
        )
        every = jnp.arange(expert_count * capacity, dtype=jnp.int32)
        pick = (slot[:, None] == every[None, :]).astype(BF16)
        return jnp.dot(pick, returned, preferred_element_type=F32) * route_weight[:, k : k + 1]

    combined = (picked(0) + picked(1)).astype(BF16)
    groups = [list(range(side, tp_size, 2)) for side in range(2)]
    expert_out = lax.psum_scatter(
        combined, "tp", scatter_dimension=1, axis_index_groups=groups, tiled=True
    )
    return (mixer_out, expert_out)


def solution(mesh):
    return jax.shard_map(
        local,
        mesh=mesh,
        in_specs=(
            P("ep", None),
            P("ep", None),
            P("ep", None),
            P(),
            P(),
            P(None, "tp"),
            P(None, "tp"),
            P(None, "tp"),
            P(None, "tp"),
            P("tp", None),
            P("ep", None),
            P(),
            P("ep", None),
            P("ep", None),
            P("ep", None, "tp"),
            P("ep", None, "tp"),
            P("ep", "tp", None),
        ),
        out_specs=(P(("ep", "tp"), None), P("ep", "tp")),
        check_vma=False,
    )
```

profile of v0, /device:TPU:0, one launch (start us, length us, event | category | flops | bytes accessed | tf_op | source)
XLA Modules:
  0.0 209.3 jit_solution(14046167022091732898)
XLA Ops:
  7.3 2.2 %copy.26 = bf16[512,512]{0,1:T(8,128)(2,1)} copy(bf16[512,512]{1,0:T(8,128)(2,1)} %param.18) | data formatting | bytes 1048576 | tf_op args[1]
  9.5 2.2 %convert_element_type.109 = f32[512,512]{0,1:T(8,128)} convert(bf16[512,512]{0,1:T(8,128)(2,1)} %copy.26) | non-fusion elementwise | flops 262144 | bytes 1572864 | tf_op jit(solution)/shard_map/convert_element_type | solution.py:20
  15.3 2.5 %convert_element_type.115 = f32[512,2048]{1,0:T(8,128)} convert(bf16[512,2048]{1,0:T(8,128)(2,1)S(1)} %copy-done.1) | non-fusion elementwise | flops 1048576 | bytes 6291456 | tf_op jit(solution)/shard_map/convert_element_type | solution.py:20
  21.6 3.5 %convolution_convert_fusion = bf16[1536,1024]{1,0:T(8,128)(2,1)} fusion(pred[1536,512]{1,0:T(32,128)(4,1)S(1)} %bitcast_compare_fusion, bf16[512,1024]{1,0:T(8,128)(2,1)S(1)} %fusion.12), kind=kOutput, calls=%fused_computation.3 | convolution fusion | flops 1612185600 | bytes 4980736 | tf_op jit(solution)/shard_map/dot_general | solution.py:208
  25.0 5.3 %all-to-all-start = ((bf16[4,2,192,1024]{3,2,1,0:T(8,128)(2,1)}), bf16[4,2,192,1024]{3,2,1,0:T(8,128)(2,1)}, u32[]{:S(2)}, u32[]{:S(2)}) async-start(bf16[4,2,192,1024]{3,2,1,0:T(8,128)(2,1)} %bitcast.92), calls=%async_computation | async-start | bytes 6291456 | tf_op jit(solution)/shard_map/all_to_all | solution.py:210
  32.6 31.8 %all-gather.2.cloned.1.call-done = bf16[2048,288]{0,1:T(8,128)(2,1)} async-done(((bf16[512,288]{0,1:T(8,128)(2,1)}), bf16[2048,288]{0,1:T(8,128)(2,1)}) %all-gather.2.cloned.1.call-update) | async-done | bytes 1179664 | tf_op jit(solution)/shard_map/all_gather | solution.py:195
  65.8 2.4 %fusion.44.qt_ref = bf16[512,128]{1,0:T(8,128)(2,1)S(1)} fusion(f32[512,128]{1,0:T(8,128)} %convolution_multiply_fusion, bf16[1024,128]{1,0:T(8,128)(2,1)} %param.23, f32[128]{0:T(128)S(1)} %get-tuple-element.25, f32[128]{0:T(128)S(1)} %get-tuple-element.26, f32[512]{0:T(512)S(1)} %add_convert_fusion.1, s32[128]{0:T(128)S(1)} %fusion.69, ...), kind=kOutput, calls=%fused_computation.65 | convolution fusion | flops 170360832 | bytes 1713664 | tf_op jit(solution)/shard_map/dot_general | solution.py:141
  70.7 2.5 %fusion.7.kt_ref = bf16[256,2048]{1,0:T(8,128)(2,1)S(1)} fusion(bf16[512,256]{1,0:T(8,128)(2,1)} %param.24, bf16[2048,256]{0,1:T(8,128)(2,1)} %collective-permute-done, bf16[2048,256]{0,1:T(8,128)(2,1)S(1)} %slice.28, pred[]{:T(512)S(6)} %eq.151), kind=kOutput, calls=%fused_computation.22 | convolution fusion | flops 546832384 | bytes 3407873 | tf_op jit(solution)/shard_map/td,df->ft/dot_general | solution.py:149
  73.3 2.5 %convolution_convert_fusion.2.v_ref = bf16[2048,256]{1,0:T(8,128)(2,1)S(1)} fusion(bf16[512,256]{1,0:T(8,128)(2,1)S(1)} %copy-done.10, bf16[2048,256]{0,1:T(8,128)(2,1)} %collective-permute-done, bf16[2048,256]{0,1:T(8,128)(2,1)S(1)} %slice.28, pred[]{:T(512)S(6)} %eq.151), kind=kOutput, calls=%fused_computation.20 | convolution fusion | flops 546832384 | bytes 3407873 | tf_op jit(solution)/shard_map/dot_general | solution.py:150
  75.7 9.7 %attention.1 = bf16[512,256]{1,0:T(8,128)(2,1)S(1)} custom-call(bf16[512,256]{1,0:T(8,128)(2,1)S(1)} %convolution_convert_fusion.5.q_ref, bf16[512,128]{1,0:T(8,128)(2,1)S(1)} %fusion.44.qt_ref, bf16[256,2048]{1,0:T(8,128)(2,1)S(1)} %fusion.7.kt_ref, bf16[32,2048]{1,0:T(8,128)(2,1)S(1)} %slice_bitcast_fusion.tk_ref, ...), custom_call_target="tpu_custom_call" | custom-call | flops 16106127360 | bytes 2097152 | tf_op jit(solution)/shard_map/attention/pallas_call | solution.py:75
  85.5 3.9 %copy.28 = bf16[4,2,192,1024]{3,2,0,1:T(8,128)(2,1)} copy(bf16[4,2,192,1024]{3,2,1,0:T(8,128)(2,1)} %all-to-all-done) | data formatting | bytes 6291456 | tf_op jit(solution)/shard_map/optimization_barrier | solution.py:223
  89.9 2.7 %constant_dynamic-slice_fusion.7 = (bf16[2,512,256]{2,1,0:T(8,128)(2,1)S(1)}, bf16[2,512,256]{2,1,0:T(8,128)(2,1)S(1)}, bf16[2,512,256]{2,1,0:T(8,128)(2,1)S(1)}...) fusion(bf16[2,512,2048]{2,1,0:T(8,128)(2,1)} %param.33, ...), kind=kLoop, calls=%fused_computation.109 | loop fusion | bytes 8388640 | tf_op jit(solution)/shard_map/dynamic_slice | solution.py:158
  93.4 3.8 %fusion.27 = f32[2,512,4,192]{1,3,2,0:T(8,128)S(1)} fusion(bf16[2,2048,512]{2,1,0:T(8,128)(2,1)S(1)} %copy-done.8, s32[]{:T(128)S(6)} %select_n.179, bf16[4,2,192,1024]{3,2,1,0:T(8,128)(2,1)} %all-to-all-done), kind=kOutput, calls=%fused_computation.46 | convolution fusion | flops 1610612736 | bytes 8388612 | tf_op jit(solution)/shard_map/secd,edf->secf/dot_general | solution.py:233
  97.2 3.7 %fusion.31 = f32[2,512,4,192]{1,3,2,0:T(8,128)S(1)} fusion(bf16[2,2048,512]{2,1,0:T(8,128)(2,1)S(1)} %copy-done.7, s32[]{:T(128)S(6)} %select_n.179, bf16[4,2,192,1024]{3,2,1,0:T(8,128)(2,1)} %all-to-all-done), kind=kOutput, calls=%fused_computation.50 | convolution fusion | flops 1610612736 | bytes 8388612 | tf_op jit(solution)/shard_map/secd,edf->secf/dot_general | solution.py:233
  100.9 3.7 %fusion.29 = f32[2,512,4,192]{1,3,2,0:T(8,128)S(1)} fusion(bf16[4,2,192,1024]{3,2,0,1:T(8,128)(2,1)} %collective-permute-done.1, bf16[2,2048,512]{2,1,0:T(8,128)(2,1)S(1)} %copy-done.7, s32[]{:T(128)S(6)} %select_n.192), kind=kOutput, calls=%fused_computation.48 | convolution fusion | flops 1610612736 | bytes 8388612 | tf_op jit(solution)/shard_map/secd,edf->secf/dot_general | solution.py:235
  104.6 4.3 %fusion.1 = bf16[4,2,192,512]{3,2,0,1:T(8,128)(2,1)S(1)} fusion(f32[2,512,4,192]{1,3,2,0:T(8,128)S(1)} %fusion.27, f32[2,512,4,192]{1,3,2,0:T(8,128)S(1)} %fusion.31, f32[2,512,4,192]{1,3,2,0:T(8,128)S(1)} %fusion.29, bf16[4,2,192,1024]{3,2,0,1:T(8,128)(2,1)} %collective-permute-done.1, bf16[2,2048,512]{2,1,0:T(8,128)(2,1)S(1)} %copy-done.8, s32[]{:T(128)S(6)} %select_n.192), kind=kOutput, calls=%fused_computation.5 | convolution fusion | flops 1616904192 | bytes 16252932 | tf_op jit(solution)/shard_map/secd,edf->secf/dot_general | solution.py:235
  108.9 3.2 %convert_bitcast_fusion = bf16[4,2,192,1024]{3,2,0,1:T(8,128)(2,1)} fusion(bf16[4,2,192,512]{3,2,0,1:T(8,128)(2,1)S(1)} %fusion.1, bf16[2,512,256]{2,1,0:T(8,128)(2,1)S(1)} %get-tuple-element.18, bf16[2,512,256]{2,1,0:T(8,128)(2,1)S(1)} %get-tuple-element.19, bf16[2,512,256]{2,1,0:T(8,128)(2,1)S(1)} %get-tuple-element.13, ...), kind=kOutput, calls=%fused_computation.13 | convolution fusion | flops 1620574208 | bytes 6815744 | tf_op jit(solution)/shard_map/secf,efd->secd/dot_general | solution.py:244
  114.2 3.9 %collective-permute-done.2 = bf16[4,2,192,1024]{3,2,0,1:T(8,128)(2,1)} collective-permute-done((bf16[4,2,192,1024]{3,2,0,1:T(8,128)(2,1)}, bf16[4,2,192,1024]{3,2,0,1:T(8,128)(2,1)}, u32[]{:S(2)}, u32[]{:S(2)}) %collective-permute-start.2) | collective-permute-done | bytes 3145760 | tf_op jit(solution)/shard_map/ppermute | solution.py:104
  118.1 4.6 %fusion = bf16[4,2,192,1024]{3,2,0,1:T(8,128)(2,1)S(1)} fusion(bf16[4,2,192,1024]{3,2,0,1:T(8,128)(2,1)} %collective-permute-done.2, bf16[4,2,192,512]{3,2,0,1:T(8,128)(2,1)} %copy-done.13, bf16[2,512,256]{2,1,0:T(8,128)(2,1)S(1)} %get-tuple-element.15, bf16[2,512,256]{2,1,0:T(8,128)(2,1)S(1)} %get-tuple-element.16, ...), kind=kOutput, calls=%fused_computation.1 | convolution fusion | flops 1626865664 | bytes 9961472 | tf_op jit(solution)/shard_map/secf,efd->secd/dot_general | solution.py:244
  124.7 4.8 %all-to-all-start.1 = ((bf16[4,2,192,1024]{3,2,1,0:T(8,128)(2,1)}), bf16[4,2,192,1024]{3,2,1,0:T(8,128)(2,1)}, u32[]{:S(2)}, u32[]{:S(2)}) async-start(bf16[4,2,192,1024]{3,2,1,0:T(8,128)(2,1)} %copy.31), calls=%async_computation.2 | async-start | bytes 6291456 | tf_op jit(solution)/shard_map/all_to_all | solution.py:253
  129.5 36.7 %all-to-all-done.1 = bf16[4,2,192,1024]{3,2,1,0:T(8,128)(2,1)} async-done(((bf16[4,2,192,1024]{3,2,1,0:T(8,128)(2,1)}), bf16[4,2,192,1024]{3,2,1,0:T(8,128)(2,1)}, u32[]{:S(2)}, u32[]{:S(2)}) %all-to-all-start.1) | async-done | bytes 3145760 | tf_op jit(solution)/shard_map/all_to_all | solution.py:253
  166.2 3.7 %fusion.5 = f32[512,1024]{1,0:T(8,128)S(1)} fusion(bf16[1536,1024]{1,0:T(8,128)(2,1)} %bitcast.24, s32[512]{0:T(512)S(1)} %copy-done.15), kind=kOutput, calls=%fused_computation.15 | convolution fusion | flops 1611399168 | bytes 5244928 | tf_op jit(solution)/shard_map/dot_general | solution.py:263
  169.9 4.8 %add_convert_fusion = bf16[512,1024]{1,0:T(8,128)(2,1)} fusion(f32[512,1024]{1,0:T(8,128)S(1)} %fusion.5, bf16[1536,1024]{1,0:T(8,128)(2,1)} %bitcast.24, s32[512]{0:T(512)S(1)} %copy-done.14, f32[512]{0:T(512)S(1)} %bitcast.95, f32[512]{0:T(512)S(1)} %bitcast.94), kind=kOutput, calls=%fused_computation.52 | convolution fusion | flops 1613496320 | bytes 6297600 | tf_op jit(solution)/shard_map/dot_general | solution.py:263
  174.8 27.9 %reduce-scatter.5.cloned.1.call-done = bf16[512,256]{1,0:T(8,128)(2,1)} async-done(((bf16[512,1024]{1,0:T(8,128)(2,1)}), bf16[512,256]{1,0:T(8,128)(2,1)}) %reduce-scatter.5.cloned.1.call-update) | async-done | bytes 262160 | tf_op jit(solution)/shard_map/reduce_scatter | solution.py:267
  (75 shorter events, 18.9 us)
Async XLA Ops:
  7.2 105.0 %copy-start = (bf16[256,2048]{1,0:T(8,128)(2,1)S(1)}, bf16[256,2048]{1,0:T(8,128)(2,1)}, u32[]{:S(2)}) copy-start(bf16[256,2048]{1,0:T(8,128)(2,1)} %param.26) | copy-start | bytes 3145732
  7.2 5.7 %copy-start.6 = (f32[512]{0:T(512)S(1)}, f32[512]{0:T(512)}, u32[]{:S(2)}) copy-start(f32[512]{0:T(512)} %param.21) | copy-start | bytes 6148
  7.2 7.0 %copy-start.11 = (bf16[512,32]{0,1:T(8,128)(2,1)S(1)}, bf16[512,32]{0,1:T(8,128)(2,1)}, u32[]{:S(2)}) copy-start(bf16[512,32]{0,1:T(8,128)(2,1)} %param.19) | copy-start | bytes 98308
  7.2 8.1 %copy-start.1 = (bf16[512,2048]{1,0:T(8,128)(2,1)S(1)}, bf16[512,2048]{1,0:T(8,128)(2,1)}, u32[]{:S(2)}) copy-start(bf16[512,2048]{1,0:T(8,128)(2,1)} %param.27) | copy-start | bytes 6291460
  7.2 57.2 %all-gather.2.cloned.1.call-start = ((), (), s32[]{:S(2)}) async-start(), calls=%async_computation.4 | async-start | bytes 1474560 | tf_op jit(solution)/shard_map/all_gather | solution.py:195
  15.3 3.0 %copy-start.5 = (f32[2048]{0:T(1024)S(1)}, f32[2048]{0:T(1024)}, u32[]{:S(2)}) copy-start(f32[2048]{0:T(1024)} %param.28) | copy-start | bytes 24580
  17.8 2.5 %copy-start.3 = (s32[512,2]{0,1:T(2,128)S(1)}, s32[512,2]{0,1:T(2,128)}, u32[]{:S(2)}) copy-start(s32[512,2]{0,1:T(2,128)} %param.29) | copy-start | bytes 12292
  25.0 5.3 %copy-start.2 = (bf16[512,1024]{1,0:T(8,128)(2,1)S(1)}, bf16[512,1024]{1,0:T(8,128)(2,1)}, u32[]{:S(2)}) copy-start(bf16[512,1024]{1,0:T(8,128)(2,1)} %param.17) | copy-start | bytes 3145732
  25.0 5.6 %copy-start.9 = (bf16[1024,128]{1,0:T(8,128)(2,1)S(1)}, bf16[1024,128]{1,0:T(8,128)(2,1)}, u32[]{:S(2)}) copy-start(bf16[1024,128]{1,0:T(8,128)(2,1)} %param.23) | copy-start | bytes 786436
  25.0 5.6 %copy-start.12 = (f32[1024]{0:T(1024)S(1)}, f32[1024]{0:T(1024)}, u32[]{:S(2)}) copy-start(f32[1024]{0:T(1024)} %param.20) | copy-start | bytes 12292
  25.0 60.4 %all-to-all-start = ((bf16[4,2,192,1024]{3,2,1,0:T(8,128)(2,1)}), bf16[4,2,192,1024]{3,2,1,0:T(8,128)(2,1)}, u32[]{:S(2)}, u32[]{:S(2)}) async-start(bf16[4,2,192,1024]{3,2,1,0:T(8,128)(2,1)} %bitcast.92), calls=%async_computation | async-start | bytes 6291456 | tf_op jit(solution)/shard_map/all_to_all | solution.py:210
  30.4 144.4 %reduce-scatter.3.cloned.1.call-start = ((), (), s32[]{:S(2)}) async-start(), calls=%async_computation.5 | async-start | bytes 2359296 | tf_op jit(solution)/shard_map/reduce_scatter | solution.py:225
  65.7 5.0 %collective-permute-start = (bf16[2048,256]{0,1:T(8,128)(2,1)S(1)}, bf16[2048,256]{0,1:T(8,128)(2,1)}, u32[]{:S(2)}, u32[]{:S(2)}) collective-permute-start(bf16[2048,256]{0,1:T(8,128)(2,1)S(1)} %slice.28), channel_id=1, source_target_pairs={{0,1},{1,0},{2,3},{3,2},{4,5},{5,4},{6,7},{7,6},{8,9},{9,8},{10,11... | collective-permute-start | bytes 3145736 | tf_op jit(solution)/shard_map/ppermute | solution.py:104
  70.7 2.6 %copy-start.10 = (bf16[512,256]{1,0:T(8,128)(2,1)S(1)}, bf16[512,256]{1,0:T(8,128)(2,1)}, u32[]{:S(2)}) copy-start(bf16[512,256]{1,0:T(8,128)(2,1)} %param.25) | copy-start | bytes 786436
  89.4 11.5 %collective-permute-start.1 = (bf16[4,2,192,1024]{3,2,0,1:T(8,128)(2,1)}, bf16[4,2,192,1024]{3,2,0,1:T(8,128)(2,1)}, u32[]{:S(2)}, u32[]{:S(2)}) collective-permute-start(bf16[4,2,192,1024]{3,2,0,1:T(8,128)(2,1)} %copy.28), channel_id=1, source_target_pairs={{0,1},{1,0},{2,3},{3,2},{4,5},{5,4},{6,7},{7,6},{8,9},{9,8},{10,11... | collective-permute-start | bytes 9437192 | tf_op jit(solution)/shard_map/ppermute | solution.py:104
  89.9 3.5 %copy-start.8 = (bf16[2,2048,512]{2,1,0:T(8,128)(2,1)S(1)}, bf16[2,2048,512]{2,1,0:T(8,128)(2,1)}, u32[]{:S(2)}) copy-start(bf16[2,2048,512]{2,1,0:T(8,128)(2,1)} %param.32) | copy-start | bytes 12582916
  93.4 3.8 %copy-start.7 = (bf16[2,2048,512]{2,1,0:T(8,128)(2,1)S(1)}, bf16[2,2048,512]{2,1,0:T(8,128)(2,1)}, u32[]{:S(2)}) copy-start(bf16[2,2048,512]{2,1,0:T(8,128)(2,1)} %param.31) | copy-start | bytes 12582916
  108.9 3.2 %copy-start.13 = (bf16[4,2,192,512]{3,2,0,1:T(8,128)(2,1)}, bf16[4,2,192,512]{3,2,0,1:T(8,128)(2,1)S(1)}, u32[]{:S(2)}) copy-start(bf16[4,2,192,512]{3,2,0,1:T(8,128)(2,1)S(1)} %fusion.1) | copy-start | bytes 4718596
  112.1 6.0 %collective-permute-start.2 = (bf16[4,2,192,1024]{3,2,0,1:T(8,128)(2,1)}, bf16[4,2,192,1024]{3,2,0,1:T(8,128)(2,1)}, u32[]{:S(2)}, u32[]{:S(2)}) collective-permute-start(bf16[4,2,192,1024]{3,2,0,1:T(8,128)(2,1)} %convert_bitcast_fusion), channel_id=1, source_target_pairs={{0,1},{1,0},{2,3},{3,2},{4,5},{5,4},{6,7},{7,6},{8,9},{9,8},{10,11... | collective-permute-start | bytes 9437192 | tf_op jit(solution)/shard_map/ppermute | solution.py:104
  124.6 4.9 %copy-start.4 = (f32[512,2]{0,1:T(2,128)S(1)}, f32[512,2]{0,1:T(2,128)}, u32[]{:S(2)}) copy-start(f32[512,2]{0,1:T(2,128)} %param.30) | copy-start | bytes 12292
  124.7 41.5 %copy-start.15 = (s32[512]{0:T(512)S(1)}, s32[512]{0:T(512)}, u32[]{:S(2)}) copy-start(s32[512]{0:T(512)} %get-tuple-element.11) | copy-start | bytes 6148
  124.7 41.5 %all-to-all-start.1 = ((bf16[4,2,192,1024]{3,2,1,0:T(8,128)(2,1)}), bf16[4,2,192,1024]{3,2,1,0:T(8,128)(2,1)}, u32[]{:S(2)}, u32[]{:S(2)}) async-start(bf16[4,2,192,1024]{3,2,1,0:T(8,128)(2,1)} %copy.31), calls=%async_computation.2 | async-start | bytes 6291456 | tf_op jit(solution)/shard_map/all_to_all | solution.py:253
  129.5 73.3 %reduce-scatter.5.cloned.1.call-start = ((), (), s32[]{:S(2)}) async-start(), calls=%async_computation.6 | async-start | bytes 1310720 | tf_op jit(solution)/shard_map/reduce_scatter | solution.py:267
  166.2 3.7 %copy-start.14 = (s32[512]{0:T(512)S(1)}, s32[512]{0:T(512)}, u32[]{:S(2)}) copy-start(s32[512]{0:T(512)} %get-tuple-element.10) | copy-start | bytes 6148
Sparse Core Ops, SparseCore 0:
  15.4 49.0 all-gather.1
  114.3 35.7 reduce-scatter.2
  174.9 27.7 reduce-scatter.4
where the time goes:
time: 210 us; the launch traced here: 209 us
  waiting for transfers between devices  100 us (48%)
  matrix products  49.3 us (23%)
  between operations  14.2 us (7%)
  local copies, waits for them, and re-layouts  14 us (7%)
  other arithmetic  10.9 us (5%)
  starting transfers between devices  10.8 us (5%)
  Pallas kernels  9.74 us (5%)
    all_to_all x1, waiting for transfers between devices, local(): lax.all_to_all(summed, 'ep', split_axis=0, concat_axis=0, tiled=True)  36.7 us
    all_gather x1, waiting for transfers between devices, local(): gathered = lax.all_gather(part, 'ep', axis=0, tiled=True)  31.8 us
    reduce_scatter x1, waiting for transfers between devices, local(): lax.psum_scatter(combined, 'tp', scatter_dimension=1, axis_index_groups=g...  27.9 us
    pallas_call x1, Pallas kernels, attention(): pl.pallas_call(functools.partial(attention_kernel, head_count, turn_width...  9.74 us
    dot_general x2, matrix products, picked(): jnp.dot(pick, returned, preferred_element_type=F32)  8.54 us
    dot_general x2, matrix products, project(): jnp.einsum('secd,edf->secf', other, half_of(weight, 1 - parity, 1), prefe...  7.95 us
    dot_general x2, matrix products, down(): jnp.einsum('secf,efd->secd', hidden, column_blocks(down_weight, side, tp_...  7.76 us
    dot_general x2, matrix products, project(): jnp.einsum('secd,edf->secf', mine, half_of(weight, parity, 1), preferred_...  7.51 us
  transfers between devices with their start and end apart: 8, of which 4 were waited for; matrix products, arithmetic and copies ran while one was open for 24% of the time, Pallas kernels for 5%

commit v1 on v0

v1 whole, which is shorter than its diff:
```python
import functools
import math

import jax
import jax.numpy as jnp
import numpy as np
from jax import lax
from jax.experimental import pallas as pl
from jax.experimental.pallas import tpu as pltpu
from jax.sharding import PartitionSpec as P

NOPE = 64
VDIM = 64

NORM_EPSILON = 1e-06
ROTARY_BASE = 10000.0
F32 = jnp.float32
BF16 = jnp.bfloat16
MESH = pl.DeviceIdType.MESH
EARLY = 1


def xor(a, b, size):
    total, weight = 0, 1
    while weight < size:
        total = total + weight * ((a // weight + b // weight) % 2)
        weight *= 2
    return total


def dot(a, b):
    return jnp.dot(a, b, preferred_element_type=F32)


def dot_nt(a, b):
    return lax.dot_general(a, b, (((1,), (1,)), ((), ())), preferred_element_type=F32)


def iota(shape, axis):
    return lax.broadcasted_iota(jnp.int32, shape, axis)


def norm_factor(square_sum, width):
    return lax.rsqrt(square_sum * (1.0 / width) + NORM_EPSILON)


def kernel(
    dims,
    routes_ref,
    weights_ref,
    rotary_ref,
    freq_col_ref,
    freq_row_ref,
    query_gain_ref,
    joint_gain_ref,
    expert_gain_ref,
    query_latent_hbm,
    joint_hbm,
    query_weight_hbm,
    query_rotary_hbm,
    key_weight_hbm,
    value_weight_hbm,
    output_weight_hbm,
    expert_hbm,
    gate_hbm,
    up_hbm,
    down_hbm,
    mixer_ref,
    expert_out_ref,
    query_latent,
    joint,
    query_weight,
    query_rotary,
    key_weight,
    value_weight,
    output_weight,
    expert_in,
    gate,
    up,
    down,
    table,
    rows_half,
    outgoing,
    slots,
    pick,
    turned,
    queries,
    keys,
    values,
    attended,
    partial,
    mixer_pair,
    mixer_in,
    ours,
    theirs,
    arrived,
    returned,
    combined,
    combined_in,
    load_sem,
    joint_send,
    joint_recv,
    joint_core_send,
    joint_core_recv,
    turned_send,
    turned_recv,
    out_send,
    out_recv,
    core_send,
    core_recv,
    pair_send,
    pair_recv,
    mixer_send,
    mixer_recv,
    half_send,
    half_recv,
    back_send,
    back_recv,
    line_send,
    line_recv,
):
    n, m, rows, width, local_count, capacity, head_count, turn = dims
    nz = m // 2
    experts = n * local_count
    half = width // 2
    block_width = width // m
    row_block = rows // m
    hidden_width = gate.shape[2]
    latent_width = joint_hbm.shape[1]
    latent_half = latent_width // 2
    tokens = n * rows
    batch = local_count * capacity
    half_turn = turn // 2

    me = lax.axis_index("ep")
    t = lax.axis_index("tp")
    z = t // 2
    c = t % 2

    def at_ep(step):
        return (xor(me, step, n), t)

    def at_z(step):
        return (me, 2 * xor(z, step, nz) + c)

    partner = (me, 2 * z + 1 - c)

    def remote(src, dst, send, recv, where):
        return pltpu.make_async_remote_copy(
            src_ref=src, dst_ref=dst, send_sem=send, recv_sem=recv, device_id=where, device_id_type=MESH
        )

    loads = [
        pltpu.make_async_copy(src, dst, load_sem.at[i])
        for i, (src, dst) in enumerate(
            [
                (expert_hbm, expert_in),
                (joint_hbm.at[:, pl.ds(0, latent_half)], joint.at[0, 0]),
                (joint_hbm.at[:, pl.ds(latent_half, latent_half)], joint.at[1, 0]),
                (query_latent_hbm, query_latent),
                (query_weight_hbm, query_weight),
                (query_rotary_hbm, query_rotary),
                (key_weight_hbm, key_weight),
                (value_weight_hbm, value_weight),
                (output_weight_hbm, output_weight),
                (gate_hbm, gate),
                (up_hbm, up),
                (down_hbm, down),
            ]
        )
    ]
    for load in loads:
        load.start()

    barrier = pltpu.get_barrier_semaphore()
    peers = [at_ep(step) for step in range(1, n)] + [at_z(step) for step in range(1, nz)] + [partner]
    for peer in peers:
        pl.semaphore_signal(barrier, inc=1, device_id=peer, device_id_type=MESH)
    pl.semaphore_wait(barrier, len(peers))

    joint_half = joint_hbm.at[:, pl.ds(pl.multiple_of(c * latent_half, latent_half), latent_half)]
    joint_copies = [
        remote(joint_half, joint.at[c, step], joint_send.at[step], joint_recv.at[step], at_ep(step))
        for step in range(1, n)
    ]
    for copy in joint_copies:
        copy.start()

    position = (me * rows + iota((half_turn, rows), 1)).astype(F32)
    angle = position * freq_col_ref[...]
    cosine, sine = jnp.cos(angle), jnp.sin(angle)
    first = rotary_ref[0:half_turn, :].astype(F32)
    second = rotary_ref[half_turn:turn, :].astype(F32)
    turned[0] = jnp.concatenate(
        [first * cosine - second * sine, second * cosine + first * sine], axis=0
    ).astype(BF16)

    names = iota((experts, rows), 0)
    first_member = routes_ref[0:1, :] == names
    second_member = routes_ref[1:2, :] == names
    member = first_member | second_member
    before = (iota((rows, rows), 0) < iota((rows, rows), 1)).astype(BF16)
    rank = dot(member.astype(BF16), before)
    place = jnp.where(member, rank, -4096.0)
    share = jnp.where(first_member, weights_ref[0:1, :], 0.0) + jnp.where(
        second_member, weights_ref[1:2, :], 0.0
    )
    table[...] = jnp.zeros_like(table)
    for group in range(n):
        span = slice(group * local_count, (group + 1) * local_count)
        table[group, 0:local_count, :] = place[span, :]
        table[group, local_count : 2 * local_count, :] = share[span, :]

    turned_copies = [
        remote(turned.at[0], turned.at[step], turned_send.at[step], turned_recv.at[step], at_ep(step))
        for step in range(1, n)
    ]
    for copy in turned_copies:
        copy.start()

    loads[0].wait()
    piece = 128 if rows % 128 == 0 else rows
    own_columns = pl.ds(pl.multiple_of(c * half, half), half)

    @pl.loop(0, rows // piece)
    def _(i):
        span = pl.ds(pl.multiple_of(i * piece, piece), piece)
        whole = expert_in[span, :].astype(F32)
        factor = norm_factor(jnp.sum(whole * whole, axis=-1, keepdims=True), width)
        part = expert_in[span, own_columns].astype(F32)
        rows_half[span, :] = (part * factor * expert_gain_ref[:, own_columns]).astype(BF16)

    def chosen(step, expert):
        group = xor(me, step, n)
        spots = table[group, expert : expert + 1, :]
        hit = iota((capacity, rows), 0).astype(F32) == spots
        return dot(hit.astype(BF16), rows_half[...]).astype(BF16)

    out_copies = []
    for step in range(1, n):
        for expert in range(local_count):
            outgoing[step - 1, expert] = chosen(step, expert)
        copy = remote(
            outgoing.at[step - 1],
            slots.at[c, :, pl.ds(step * capacity, capacity), :],
            out_send.at[step],
            out_recv.at[step],
            at_ep(step),
        )
        copy.start()
        out_copies.append(copy)
    for expert in range(local_count):
        slots[c, expert, 0:capacity, :] = chosen(0, expert)

    def core_copy(step):
        where = (c, slice(None), pl.ds(step * capacity, capacity), slice(None))
        return remote(slots.at[where], slots.at[where], core_send.at[step], core_recv.at[step], partner)

    core_copies = [core_copy(step) for step in range(n)]
    core_copies[0].start()

    same = (iota((rows, rows), 0) == iota((rows, rows), 1)).astype(BF16)

    @pl.loop(0, n)
    def _(step):
        group = xor(me, step, n)
        upright = dot_nt(same, table[group].astype(BF16))
        lane = iota((rows, batch), 1).astype(F32)
        total = jnp.zeros((rows, batch), F32)
        for expert in range(local_count):
            spot = upright[:, expert : expert + 1] + float(expert * capacity)
            gain = upright[:, local_count + expert : local_count + expert + 1]
            total = total + jnp.where(lane == spot, gain, 0.0)
        pick[step] = total.astype(BF16)

    for i in (3, 4, 5):
        loads[i].wait()
    turn_width = head_count * turn
    lane = iota((turn_width, turn_width), 0)
    other = iota((turn_width, turn_width), 1)
    other = (other // turn) * turn + (other % turn + half_turn) % turn
    swapped = dot(query_rotary[...], (lane == other).astype(BF16)).astype(BF16)
    query_width = query_latent.shape[1]

    @pl.loop(0, rows // piece)
    def _(i):
        span = pl.ds(pl.multiple_of(i * piece, piece), piece)
        source = query_latent[span, :].astype(F32)
        factor = norm_factor(jnp.sum(source * source, axis=-1, keepdims=True), query_width)
        normed = (source * factor * query_gain_ref[...]).astype(BF16)
        plain = dot(normed, query_weight[...]).astype(BF16)
        at = (me * rows + i * piece + iota((piece, turn_width), 0)).astype(F32) * freq_row_ref[...]
        sign = jnp.where(iota((piece, turn_width), 1) % turn < half_turn, -1.0, 1.0)
        spun = dot(normed, query_rotary[...]) * jnp.cos(at) + dot(normed, swapped) * (jnp.sin(at) * sign)
        spun = spun.astype(BF16)
        for head in range(head_count):
            queries[head, span, :] = jnp.concatenate(
                [plain[:, head * NOPE : (head + 1) * NOPE], spun[:, head * turn : (head + 1) * turn]],
                axis=1,
            )

    def joint_core(step):
        here = joint.at[c, step]
        return remote(here, here, joint_core_send.at[step], joint_core_recv.at[step], partner)

    joint_cores = [joint_core(step) for step in range(1, n)]
    for i in (1, 2, 6, 7):
        loads[i].wait()
    key_turned = jnp.transpose(key_weight[...].astype(F32)).astype(BF16)

    def keys_of(step):
        left = joint[0, step].astype(F32)
        right = joint[1, step].astype(F32)
        square = jnp.sum(left * left, axis=-1, keepdims=True) + jnp.sum(right * right, axis=-1, keepdims=True)
        factor = norm_factor(square, latent_width)
        left = (left * factor * joint_gain_ref[:, 0:latent_half]).astype(BF16)
        right = (right * factor * joint_gain_ref[:, latent_half:latent_width]).astype(BF16)
        normed = jnp.concatenate([left, right], axis=1)
        upright = dot_nt(key_turned, normed).astype(BF16)
        columns = slice(step * rows, (step + 1) * rows)
        for head in range(head_count):
            keys[head, 0:NOPE, columns] = upright[head * NOPE : (head + 1) * NOPE, :]
            keys[head, NOPE : NOPE + turn, columns] = turned[step]
        values[columns, :] = dot(normed, value_weight[...]).astype(BF16)

    keys_of(0)
    for step in range(1, n):
        joint_copies[step - 1].wait_recv()
        joint_cores[step - 1].start()
    for step in range(1, n):
        turned_copies[step - 1].wait_recv()
        joint_cores[step - 1].wait_recv()
        keys_of(step)

    scale = (NOPE + turn) ** (-0.5) * math.log2(math.e)
    query_block = max(32, min(rows, 128 * 2048 // tokens))
    per_pair = 128 // VDIM

    @pl.loop(0, rows // query_block)
    def _(i):
        span = pl.ds(pl.multiple_of(i * query_block, query_block), query_block)
        pieces = []
        for head in range(head_count):
            scores = dot(queries[head, span, :], keys[head])
            top = jnp.max(scores, axis=-1, keepdims=True)
            expo = jnp.exp2((scores - top) * scale)
            total = jnp.sum(expo, axis=-1, keepdims=True)
            pair = head // per_pair
            mixed = dot(expo.astype(BF16), values[:, pair * 128 : (pair + 1) * 128])
            inner = head % per_pair
            pieces.append((mixed[:, inner * VDIM : (inner + 1) * VDIM] / total).astype(BF16))
        attended[span, :] = jnp.concatenate(pieces, axis=1)

    loads[8].wait()
    chunk = 512

    @pl.loop(0, width // chunk)
    def _(i):
        columns = pl.ds(pl.multiple_of(i * chunk, chunk), chunk)
        product = dot(attended[...], output_weight[:, columns]).astype(BF16)
        partial[:, :, columns] = product.reshape(m, row_block, chunk)

    pair_copies = [
        remote(partial.at[2 * i + 1 - c], mixer_pair.at[i], pair_send.at[i], pair_recv.at[i], partner)
        for i in range(nz)
    ]
    for copy in pair_copies:
        copy.start()

    for step in range(1, n - 1):
        out_copies[step - 1].wait_recv()
        core_copies[step].start()

    for i in range(nz):
        pair_copies[i].wait_recv()
        both = partial[2 * i + c].astype(F32) + mixer_pair[i].astype(F32)
        mixer_pair[i] = both.astype(BF16)
    mixer_copies = [
        remote(
            mixer_pair.at[xor(z, step, nz)],
            mixer_in.at[step],
            mixer_send.at[step],
            mixer_recv.at[step],
            at_z(step),
        )
        for step in range(1, nz)
    ]
    for copy in mixer_copies[::-1]:
        copy.start()

    for i in (9, 10, 11):
        loads[i].wait()

    def experts_on(low, high):
        count = (high - low) * capacity
        span = slice(low * capacity, high * capacity)

        @pl.loop(0, local_count)
        def _(expert):
            left = slots[0, expert, span, :]
            right = slots[1, expert, span, :]
            gate_acts = dot(left, gate[expert, 0:half, :]) + dot(right, gate[expert, half:width, :])
            up_acts = dot(left, up[expert, 0:half, :]) + dot(right, up[expert, half:width, :])
            hidden = (gate_acts / (1.0 + jnp.exp(-gate_acts)) * up_acts).astype(BF16)
            for turn_index in range(nz):
                block = xor(z, nz - 1 - turn_index, nz)
                mine = pl.ds(pl.multiple_of((2 * block + c) * block_width, block_width), block_width)
                yours = pl.ds(pl.multiple_of((2 * block + 1 - c) * block_width, block_width), block_width)
                theirs[turn_index, expert, span, :] = dot(hidden, down[expert, :, yours]).astype(BF16)
                ours[turn_index, expert, span, :] = dot(hidden, down[expert, :, mine]).astype(BF16)

    def half_copy(stage, turn_index, low, high):
        where = (turn_index, slice(None), pl.ds(low * capacity, (high - low) * capacity), slice(None))
        return remote(
            theirs.at[where],
            arrived.at[where],
            half_send.at[stage, turn_index],
            half_recv.at[stage, turn_index],
            partner,
        )

    def add_halves(turn_index, low, high):
        for expert in range(local_count):
            span = slice(low * capacity, high * capacity)
            both = ours[turn_index, expert, span, :].astype(F32) + arrived[turn_index, expert, span, :].astype(F32)
            ours[turn_index, expert, span, :] = both.astype(BF16)

    def back_copy(turn_index, step):
        return remote(
            ours.at[turn_index, :, pl.ds(step * capacity, capacity), :],
            returned.at[turn_index, step],
            back_send.at[turn_index, step],
            back_recv.at[turn_index, step],
            at_ep(step),
        )

    back_copies = [[back_copy(q, step) for step in range(1, n)] for q in range(nz)]

    core_copies[0].wait_recv()
    for step in range(1, n - 1):
        core_copies[step].wait_recv()
    experts_on(0, n - 1)
    first_halves = [half_copy(0, q, 0, n - 1) for q in range(nz)]
    for copy in first_halves:
        copy.start()
    out_copies[n - 2].wait_recv()
    core_copies[n - 1].start()
    for q in range(nz):
        first_halves[q].wait_recv()
        add_halves(q, 0, n - 1)
        if q < EARLY:
            for step in range(1, n - 1):
                back_copies[q][step - 1].start()
    core_copies[n - 1].wait_recv()
    experts_on(n - 1, n)
    last_halves = [half_copy(1, q, n - 1, n) for q in range(nz)]
    for copy in last_halves:
        copy.start()
    for q in range(nz):
        last_halves[q].wait_recv()
        add_halves(q, n - 1, n)
        for step in range(1, n):
            if step == n - 1 or q >= EARLY:
                back_copies[q][step - 1].start()

    total = mixer_pair[z].astype(F32)
    for step in range(1, nz):
        mixer_copies[step - 1].wait_recv()
        total = total + mixer_in[step].astype(F32)
    mixer_ref[...] = total.astype(BF16)

    line_copies = []
    last = None
    for q in range(nz):
        own = ours[q, :, 0:capacity, :].reshape(batch, block_width)
        last = dot(pick[0], own)
        for step in range(1, n):
            back_copies[q][step - 1].wait_recv()
            last = last + dot(pick[step], returned[q, step].reshape(batch, block_width))
        if q < nz - 1:
            combined[q] = last.astype(BF16)
            step = nz - 1 - q
            copy = remote(combined.at[q], combined_in.at[step], line_send.at[step], line_recv.at[step], at_z(step))
            copy.start()
            line_copies.append(copy)
    for step in range(nz - 1, 0, -1):
        line_copies[nz - 1 - step].wait_recv()
        last = last + combined_in[step].astype(F32)
    expert_out_ref[...] = last.astype(BF16)

    sent = joint_copies + turned_copies + out_copies + core_copies + joint_cores + pair_copies
    sent = sent + mixer_copies + first_halves + last_halves + line_copies
    for copies in back_copies:
        sent = sent + copies
    for copy in sent:
        copy.wait_send()


def local(
    query_latent,
    joint_latent,
    rotary_key,
    query_gain,
    joint_gain,
    query_weight,
    query_rotary,
    key_weight,
    value_weight,
    output_weight,
    expert_input,
    expert_gain,
    routes,
    route_weight,
    gate_weight,
    up_weight,
    down_weight,
):
    n = lax.axis_size("ep")
    m = lax.axis_size("tp")
    nz = m // 2
    rows, width = expert_input.shape
    local_count = gate_weight.shape[0]
    capacity = 3 * rows // (2 * n)
    turn = rotary_key.shape[1]
    half_turn = turn // 2
    head_count = key_weight.shape[1] // NOPE
    latent_half = joint_latent.shape[1] // 2
    tokens = n * rows
    batch = local_count * capacity
    block_width = width // m
    row_block = rows // m
    half = width // 2
    dims = (n, m, rows, width, local_count, capacity, head_count, turn)

    powers = (ROTARY_BASE ** (-np.arange(half_turn) / half_turn)).astype(np.float32)
    freq_col = jnp.asarray(powers[:, None])
    freq_row = jnp.asarray(np.tile(powers, 2 * head_count)[None, :])

    small = [
        routes.T,
        route_weight.T,
        rotary_key.T,
        freq_col,
        freq_row,
        query_gain[None, :],
        joint_gain[None, :],
        expert_gain[None, :],
    ]
    large = [
        query_latent,
        joint_latent,
        query_weight,
        query_rotary,
        key_weight,
        value_weight,
        output_weight,
        expert_input,
        gate_weight,
        up_weight,
        down_weight,
    ]

    def like(source):
        return pltpu.VMEM(source.shape, source.dtype)

    def buffer(*shape):
        return pltpu.VMEM(shape, BF16)

    dma = pltpu.SemaphoreType.DMA
    scratch = [
        like(query_latent),
        buffer(2, n, rows, latent_half),
        like(query_weight),
        like(query_rotary),
        like(key_weight),
        like(value_weight),
        like(output_weight),
        like(expert_input),
        like(gate_weight),
        like(up_weight),
        like(down_weight),
        pltpu.VMEM((n, 8, rows), F32),
        buffer(rows, half),
        buffer(n - 1, local_count, capacity, half),
        buffer(2, local_count, n * capacity, half),
        buffer(n, rows, batch),
        buffer(n, turn, rows),
        buffer(head_count, rows, NOPE + turn),
        buffer(head_count, NOPE + turn, tokens),
        buffer(tokens, head_count * VDIM),
        buffer(rows, head_count * VDIM),
        buffer(m, row_block, width),
        buffer(nz, row_block, width),
        buffer(nz, row_block, width),
        buffer(nz, local_count, n * capacity, block_width),
        buffer(nz, local_count, n * capacity, block_width),
        buffer(nz, local_count, n * capacity, block_width),
        buffer(nz, n, local_count, capacity, block_width),
        buffer(nz - 1, rows, block_width),
        buffer(nz, rows, block_width),
        dma((12,)),
    ]
    for shape in ((n,), (n,), (n,), (n,), (n,), (nz,), (nz,), (2, nz), (nz, n), (nz,)):
        scratch += [dma(shape), dma(shape)]

    vmem = pl.BlockSpec(memory_space=pltpu.VMEM)
    anywhere = pl.BlockSpec(memory_space=pl.ANY)
    return pl.pallas_call(
        functools.partial(kernel, dims),
        in_specs=[vmem] * len(small) + [anywhere] * len(large),
        out_specs=(vmem, vmem),
        out_shape=(
            jax.ShapeDtypeStruct((row_block, width), BF16),
            jax.ShapeDtypeStruct((rows, block_width), BF16),
        ),
        scratch_shapes=scratch,
        compiler_params=pltpu.CompilerParams(
            collective_id=0, has_side_effects=True, vmem_limit_bytes=67043328
        ),
        name="whole",
    )(*small, *large)


def solution(mesh):
    return jax.shard_map(
        local,
        mesh=mesh,
        in_specs=(
            P("ep", None),
            P("ep", None),
            P("ep", None),
            P(),
            P(),
            P(None, "tp"),
            P(None, "tp"),
            P(None, "tp"),
            P(None, "tp"),
            P("tp", None),
            P("ep", None),
            P(),
            P("ep", None),
            P("ep", None),
            P("ep", None, "tp"),
            P("ep", None, "tp"),
            P("ep", "tp", None),
        ),
        out_specs=(P(("ep", "tp"), None), P("ep", "tp")),
        check_vma=False,
    )
```

time: 210 us -> 101 us (0.48)
  waiting for transfers between devices: 100 us -> 0 us
  Pallas kernels: 9.74 us -> 97 us
  matrix products: 49.3 us -> 0 us
  between operations: 14.2 us -> 0.65 us
  other arithmetic: 10.9 us -> 0 us
  starting transfers between devices: 10.8 us -> 0 us
  local copies, waits for them, and re-layouts: 14 us -> 3.34 us
    pallas_call x1, Pallas kernels: 9.74 us -> 97 us  [local(): pl.pallas_call(functools.partial(kernel, dims), in_specs=[vmem] * len(sma...]
    dot_general x17 -> x0, matrix products: 49.3 us -> none  [the longest x2 8.54 us: picked(): jnp.dot(pick, returned, preferred_element_type=F32)]
    all_to_all x2 -> x0, waiting for transfers between devices: 36.7 us -> none  [the longest x1 36.7 us: local(): lax.all_to_all(summed, 'ep', split_axis=0, concat_axis=0, tiled=True)]
    all_gather x1 -> x0, waiting for transfers between devices: 31.8 us -> none  [local(): gathered = lax.all_gather(part, 'ep', axis=0, tiled=True)]
    reduce_scatter x2 -> x0, waiting for transfers between devices: 27.9 us -> none  [the longest x1 27.9 us: local(): lax.psum_scatter(combined, 'tp', scatter_dimension=1, axis_index_groups=g...]
    all_to_all x2 -> x0, starting transfers between devices: 10.1 us -> none  [the longest x1 5.32 us: local(): lax.all_to_all(outgoing, 'ep', split_axis=0, concat_axis=0, tiled=True)]
    convert_element_type x5 -> x0, other arithmetic: 7.64 us -> none  [the longest x2 4.65 us: norm_rows(): as_float = source.astype(F32)]
    optimization_barrier x1 -> x0, local copies, waits for them, and re-layouts: 3.88 us -> none  [local(): mine, attended = lax.optimization_barrier((mine, attended))]
  transfers between devices with their start and end apart: 8 -> 0, of which waited for: 4 -> 0; matrix products, arithmetic and copies ran while one was open for 24% -> 0% of each run, Pallas kernels for 5% -> 0%
where the time goes in v1:
time: 101 us
  Pallas kernels  97 us (96%)
  local copies, waits for them, and re-layouts  3.34 us (3%)
    pallas_call x1, Pallas kernels, local(): pl.pallas_call(functools.partial(kernel, dims), in_specs=[vmem] * len(sma...  97 us
    unnamed x2, local copies, waits for them, and re-layouts  3.34 us

profile of v1, /device:TPU:0, one launch (start us, length us, event | category | flops | bytes accessed | tf_op | source)
XLA Modules:
  0.0 100.9 jit_solution(15698604048454242255)
XLA Ops:
  0.6 97.0 %whole.1 = (bf16[64,2048]{1,0:T(8,128)(2,1)}, bf16[512,256]{1,0:T(8,128)(2,1)}) custom-call(s32[2,512]{1,0:T(2,128)} %bitcast.8, f32[2,512]{1,0:T(2,128)} %bitcast.9, bf16[32,512]{1,0:T(8,128)(2,1)} %bitcast.6, f32[16,1]{1,0:T(8,128)} %constant.4.clone.freq_col_ref, f32[1,128]{1,0:T(1,128)} %constant.5.clone.freq_row_ref, f32[1,1024]{1,0:T(1,128)} %bitcast.10, ...), custom_call_target="tpu_custom_call" | custom-call | tf_op jit(solution)/shard_map/whole/pallas_call | solution.py:608
  97.6 1.7 %copy.23 = bf16[64,2048]{1,0:T(8,128)(2,1)} copy(bf16[64,2048]{1,0:T(8,128)(2,1)} %get-tuple-element.4) | data formatting | bytes 524288
  99.3 1.7 %copy.24 = bf16[512,256]{1,0:T(8,128)(2,1)} copy(bf16[512,256]{1,0:T(8,128)(2,1)} %get-tuple-element.5) | data formatting | bytes 524288

commit v2 on v1

--- a/solution.py
+++ b/solution.py
@@ -18,6 +18,8 @@
 BF16 = jnp.bfloat16
 MESH = pl.DeviceIdType.MESH
 EARLY = 1
+AHEAD = 2
+SHARED_EIGHTHS = 2
 
 
 def xor(a, b, size):
@@ -26,6 +28,19 @@
         total = total + weight * ((a // weight + b // weight) % 2)
         weight *= 2
     return total
+
+
+def low_bit(value):
+    return value & -value
+
+
+def line_order(size):
+    return list(range(size - 1, -1, -1))
+
+
+def line_sources(x, size):
+    limit = low_bit(x) if x else size
+    return [x ^ (1 << i) for i in range(size.bit_length()) if (1 << i) < limit]
 
 
 def dot(a, b):
@@ -81,6 +96,7 @@
     table,
     rows_half,
     outgoing,
+    outgoing_both,
     slots,
     pick,
     turned,
@@ -100,12 +116,18 @@
     load_sem,
     joint_send,
     joint_recv,
+    joint_line_send,
+    joint_line_recv,
     joint_core_send,
     joint_core_recv,
     turned_send,
     turned_recv,
     out_send,
     out_recv,
+    both_send,
+    both_recv,
+    share_send,
+    share_recv,
     core_send,
     core_recv,
     pair_send,
@@ -136,6 +158,8 @@
     t = lax.axis_index("tp")
     z = t // 2
     c = t % 2
+    parity = z % 2
+    order = line_order(nz)
 
     def at_ep(step):
         return (xor(me, step, n), t)
@@ -178,13 +202,44 @@
         pl.semaphore_signal(barrier, inc=1, device_id=peer, device_id_type=MESH)
     pl.semaphore_wait(barrier, len(peers))
 
-    joint_half = joint_hbm.at[:, pl.ds(pl.multiple_of(c * latent_half, latent_half), latent_half)]
+    quarter = latent_half // 2
+    lanes_mine = pl.ds(pl.multiple_of(parity * quarter, quarter), quarter)
+    lanes_other = pl.ds(pl.multiple_of((1 - parity) * quarter, quarter), quarter)
+    first_lane = c * latent_half + parity * quarter
+    joint_part = joint_hbm.at[:, pl.ds(pl.multiple_of(first_lane, quarter), quarter)]
+
     joint_copies = [
-        remote(joint_half, joint.at[c, step], joint_send.at[step], joint_recv.at[step], at_ep(step))
+        remote(
+            joint_part,
+            joint.at[c, step, :, lanes_mine],
+            joint_send.at[step],
+            joint_recv.at[step],
+            at_ep(step),
+        )
         for step in range(1, n)
     ]
-    for copy in joint_copies:
+
+    def joint_line(step):
+        here = joint.at[c, step, :, lanes_mine]
+        return remote(here, here, joint_line_send.at[step], joint_line_recv.at[step], at_z(1))
+
+    def joint_core(kind, step):
+        here = joint.at[c, step, :, lanes_other if kind else lanes_mine]
+        return remote(here, here, joint_core_send.at[kind, step], joint_core_recv.at[kind, step], partner)
+
+    joint_lines = [joint_line(step) for step in range(1, n)]
+    joint_cores = [[joint_core(kind, step) for step in range(1, n)] for kind in range(2)]
+    for copy in joint_copies[:-1]:
         copy.start()
+
+    def pass_joint(step):
+        joint_copies[step - 1].wait_recv()
+        joint_lines[step - 1].start()
+        joint_cores[0][step - 1].start()
+
+    def pass_joint_line(step):
+        joint_lines[step - 1].wait_recv()
+        joint_cores[1][step - 1].start()
 
     position = (me * rows + iota((half_turn, rows), 1)).astype(F32)
     angle = position * freq_col_ref[...]
@@ -230,48 +285,85 @@
         part = expert_in[span, own_columns].astype(F32)
         rows_half[span, :] = (part * factor * expert_gain_ref[:, own_columns]).astype(BF16)
 
-    def chosen(step, expert):
+    joint_copies[-1].start()
+
+    shared = half * SHARED_EIGHTHS // 8
+    share_mine = pl.ds(pl.multiple_of(parity * shared, shared), shared)
+    share_other = pl.ds(pl.multiple_of((1 - parity) * shared, shared), shared)
+    both_lanes = pl.ds(2 * shared, half - 2 * shared)
+
+    def chosen(step, expert, columns):
         group = xor(me, step, n)
         spots = table[group, expert : expert + 1, :]
         hit = iota((capacity, rows), 0).astype(F32) == spots
-        return dot(hit.astype(BF16), rows_half[...]).astype(BF16)
+        return dot(hit.astype(BF16), rows_half[:, columns]).astype(BF16)
+
+    def slots_at(step, lanes):
+        return slots.at[c, :, pl.ds(step * capacity, capacity), lanes]
 
     out_copies = []
     for step in range(1, n):
         for expert in range(local_count):
-            outgoing[step - 1, expert] = chosen(step, expert)
+            outgoing[step - 1, expert] = chosen(step, expert, share_mine)
         copy = remote(
             outgoing.at[step - 1],
-            slots.at[c, :, pl.ds(step * capacity, capacity), :],
+            slots_at(step, share_mine),
             out_send.at[step],
             out_recv.at[step],
             at_ep(step),
         )
+        out_copies.append(copy)
+    both_copies = []
+    for step in range(1, n):
+        for expert in range(local_count):
+            outgoing_both[step - 1, expert] = chosen(step, expert, both_lanes)
+        copy = remote(
+            outgoing_both.at[step - 1],
+            slots_at(step, both_lanes),
+            both_send.at[step],
+            both_recv.at[step],
+            at_ep(step),
+        )
+        both_copies.append(copy)
+
+    def share_copy(step):
+        here = slots_at(step, share_mine)
+        return remote(here, here, share_send.at[step], share_recv.at[step], at_z(1))
+
+    def core_copy(kind, step):
+        here = slots_at(step, (share_mine, share_other, both_lanes)[kind])
+        return remote(here, here, core_send.at[kind, step], core_recv.at[kind, step], partner)
+
+    share_copies = [share_copy(step) for step in range(1, n)]
+    core_copies = [[core_copy(kind, step) for step in range(n)] for kind in range(3)]
+
+    def pass_out(step):
+        out_copies[step - 1].wait_recv()
+        share_copies[step - 1].start()
+        core_copies[0][step].start()
+
+    def pass_share(step):
+        share_copies[step - 1].wait_recv()
+        core_copies[1][step].start()
+
+    def pass_both(step):
+        both_copies[step - 1].wait_recv()
+        core_copies[2][step].start()
+
+    def wait_core(step):
+        for kind in range(3):
+            core_copies[kind][step].wait_recv()
+
+    for expert in range(local_count):
+        slots[c, expert, 0:capacity, :] = chosen(0, expert, slice(None))
+    for kind in range(3):
+        core_copies[kind][0].start()
+    for step in range(1, n - 1):
+        pass_joint(step)
+    for copy in out_copies[:-1]:
         copy.start()
-        out_copies.append(copy)
-    for expert in range(local_count):
-        slots[c, expert, 0:capacity, :] = chosen(0, expert)
-
-    def core_copy(step):
-        where = (c, slice(None), pl.ds(step * capacity, capacity), slice(None))
-        return remote(slots.at[where], slots.at[where], core_send.at[step], core_recv.at[step], partner)
-
-    core_copies = [core_copy(step) for step in range(n)]
-    core_copies[0].start()
-
-    same = (iota((rows, rows), 0) == iota((rows, rows), 1)).astype(BF16)
-
-    @pl.loop(0, n)
-    def _(step):
-        group = xor(me, step, n)
-        upright = dot_nt(same, table[group].astype(BF16))
-        lane = iota((rows, batch), 1).astype(F32)
-        total = jnp.zeros((rows, batch), F32)
-        for expert in range(local_count):
-            spot = upright[:, expert : expert + 1] + float(expert * capacity)
-            gain = upright[:, local_count + expert : local_count + expert + 1]
-            total = total + jnp.where(lane == spot, gain, 0.0)
-        pick[step] = total.astype(BF16)
+    for copy in both_copies[:-1]:
+        copy.start()
 
     for i in (3, 4, 5):
         loads[i].wait()
@@ -299,11 +391,66 @@
                 axis=1,
             )
 
-    def joint_core(step):
-        here = joint.at[c, step]
-        return remote(here, here, joint_core_send.at[step], joint_core_recv.at[step], partner)
-
-    joint_cores = [joint_core(step) for step in range(1, n)]
+    for i in (9, 10, 11):
+        loads[i].wait()
+
+    def experts_on(low, high, first, last):
+        count = (high - low) * capacity
+        span = slice(low * capacity, high * capacity)
+
+        @pl.loop(first, last)
+        def _(expert):
+            left = slots[0, expert, span, :]
+            right = slots[1, expert, span, :]
+            gate_acts = dot(left, gate[expert, 0:half, :]) + dot(right, gate[expert, half:width, :])
+            up_acts = dot(left, up[expert, 0:half, :]) + dot(right, up[expert, half:width, :])
+            hidden = (gate_acts / (1.0 + jnp.exp(-gate_acts)) * up_acts).astype(BF16)
+            for turn_index in range(nz):
+                block = xor(z, order[turn_index], nz)
+                mine = pl.ds(pl.multiple_of((2 * block + c) * block_width, block_width), block_width)
+                yours = pl.ds(pl.multiple_of((2 * block + 1 - c) * block_width, block_width), block_width)
+                theirs[turn_index, expert, span, :] = dot(hidden, down[expert, :, yours]).astype(BF16)
+                ours[turn_index, expert, span, :] = dot(hidden, down[expert, :, mine]).astype(BF16)
+
+    stages = [(0, 1), (1, n - 1), (n - 1, n)]
+
+    def half_copy(stage, expert):
+        low, high = stages[stage]
+        where = (slice(None), expert, pl.ds(low * capacity, (high - low) * capacity), slice(None))
+        return remote(
+            theirs.at[where],
+            arrived.at[where],
+            half_send.at[stage, expert],
+            half_recv.at[stage, expert],
+            partner,
+        )
+
+    half_copies = [[half_copy(stage, expert) for expert in range(local_count)] for stage in range(3)]
+
+    def add_halves(turn_index, low, high):
+        for expert in range(local_count):
+            span = slice(low * capacity, high * capacity)
+            both = ours[turn_index, expert, span, :].astype(F32) + arrived[turn_index, expert, span, :].astype(F32)
+            ours[turn_index, expert, span, :] = both.astype(BF16)
+
+    def back_copy(turn_index, step):
+        return remote(
+            ours.at[turn_index, :, pl.ds(step * capacity, capacity), :],
+            returned.at[turn_index, step],
+            back_send.at[turn_index, step],
+            back_recv.at[turn_index, step],
+            at_ep(step),
+        )
+
+    back_copies = [[back_copy(q, step) for step in range(1, n)] for q in range(nz)]
+
+    pass_joint(n - 1)
+    out_copies[-1].start()
+    wait_core(0)
+    experts_on(0, 1, 0, local_count)
+    for expert in range(local_count):
+        half_copies[0][expert].start()
+
     for i in (1, 2, 6, 7):
         loads[i].wait()
     key_turned = jnp.transpose(key_weight[...].astype(F32)).astype(BF16)
@@ -323,22 +470,26 @@
             keys[head, NOPE : NOPE + turn, columns] = turned[step]
         values[columns, :] = dot(normed, value_weight[...]).astype(BF16)
 
+    both_copies[-1].start()
     keys_of(0)
-    for step in range(1, n):
-        joint_copies[step - 1].wait_recv()
-        joint_cores[step - 1].start()
+    for step in range(1, n - 1):
+        pass_joint_line(step)
+    for step in range(1, n - 1):
+        pass_out(step)
+    pass_joint_line(n - 1)
     for step in range(1, n):
         turned_copies[step - 1].wait_recv()
-        joint_cores[step - 1].wait_recv()
+        joint_cores[0][step - 1].wait_recv()
+        joint_cores[1][step - 1].wait_recv()
         keys_of(step)
 
     scale = (NOPE + turn) ** (-0.5) * math.log2(math.e)
-    query_block = max(32, min(rows, 128 * 2048 // tokens))
+    line_rows = 2 * row_block
+    query_block = max(32, min(line_rows, 128 * 2048 // tokens))
     per_pair = 128 // VDIM
 
-    @pl.loop(0, rows // query_block)
-    def _(i):
-        span = pl.ds(pl.multiple_of(i * query_block, query_block), query_block)
+    def attend(first, i):
+        span = pl.ds(pl.multiple_of(first + i * query_block, query_block), query_block)
         pieces = []
         for head in range(head_count):
             scores = dot(queries[head, span, :], keys[head])
@@ -351,147 +502,166 @@
             pieces.append((mixed[:, inner * VDIM : (inner + 1) * VDIM] / total).astype(BF16))
         attended[span, :] = jnp.concatenate(pieces, axis=1)
 
+    chunk = 512
+
+    def attend_line(x):
+        first = xor(z, x, nz) * line_rows
+        pl.loop(0, line_rows // query_block)(functools.partial(attend, first))
+
+    def project_line(x):
+        block = xor(z, x, nz)
+        span = pl.ds(pl.multiple_of(block * line_rows, line_rows), line_rows)
+
+        @pl.loop(0, width // chunk)
+        def _(i):
+            columns = pl.ds(pl.multiple_of(i * chunk, chunk), chunk)
+            product = dot(attended[span, :], output_weight[:, columns]).astype(BF16)
+            partial[pl.ds(2 * block, 2), :, columns] = product.reshape(2, row_block, chunk)
+
+    def pair_copy(x):
+        block = xor(z, x, nz)
+        return remote(
+            partial.at[2 * block + 1 - c], mixer_pair.at[block], pair_send.at[x], pair_recv.at[x], partner
+        )
+
+    pair_copies = [pair_copy(x) for x in range(nz)]
+
+    def pair_sum(x):
+        block = xor(z, x, nz)
+        pair_copies[x].wait_recv()
+        both = partial[2 * block + c].astype(F32) + mixer_pair[block].astype(F32)
+        mixer_pair[block] = both.astype(BF16)
+
+    for x in order[:-1]:
+        attend_line(x)
     loads[8].wait()
-    chunk = 512
-
-    @pl.loop(0, width // chunk)
-    def _(i):
-        columns = pl.ds(pl.multiple_of(i * chunk, chunk), chunk)
-        product = dot(attended[...], output_weight[:, columns]).astype(BF16)
-        partial[:, :, columns] = product.reshape(m, row_block, chunk)
-
-    pair_copies = [
-        remote(partial.at[2 * i + 1 - c], mixer_pair.at[i], pair_send.at[i], pair_recv.at[i], partner)
-        for i in range(nz)
-    ]
-    for copy in pair_copies:
-        copy.start()
+    for x in order[:-1]:
+        project_line(x)
+        pair_copies[x].start()
 
     for step in range(1, n - 1):
-        out_copies[step - 1].wait_recv()
-        core_copies[step].start()
-
-    for i in range(nz):
-        pair_copies[i].wait_recv()
-        both = partial[2 * i + c].astype(F32) + mixer_pair[i].astype(F32)
-        mixer_pair[i] = both.astype(BF16)
-    mixer_copies = [
-        remote(
-            mixer_pair.at[xor(z, step, nz)],
-            mixer_in.at[step],
-            mixer_send.at[step],
-            mixer_recv.at[step],
-            at_z(step),
-        )
-        for step in range(1, nz)
-    ]
-    for copy in mixer_copies[::-1]:
-        copy.start()
-
-    for i in (9, 10, 11):
-        loads[i].wait()
-
-    def experts_on(low, high):
-        count = (high - low) * capacity
-        span = slice(low * capacity, high * capacity)
-
-        @pl.loop(0, local_count)
-        def _(expert):
-            left = slots[0, expert, span, :]
-            right = slots[1, expert, span, :]
-            gate_acts = dot(left, gate[expert, 0:half, :]) + dot(right, gate[expert, half:width, :])
-            up_acts = dot(left, up[expert, 0:half, :]) + dot(right, up[expert, half:width, :])
-            hidden = (gate_acts / (1.0 + jnp.exp(-gate_acts)) * up_acts).astype(BF16)
-            for turn_index in range(nz):
-                block = xor(z, nz - 1 - turn_index, nz)
-                mine = pl.ds(pl.multiple_of((2 * block + c) * block_width, block_width), block_width)
-                yours = pl.ds(pl.multiple_of((2 * block + 1 - c) * block_width, block_width), block_width)
-                theirs[turn_index, expert, span, :] = dot(hidden, down[expert, :, yours]).astype(BF16)
-                ours[turn_index, expert, span, :] = dot(hidden, down[expert, :, mine]).astype(BF16)
-
-    def half_copy(stage, turn_index, low, high):
-        where = (turn_index, slice(None), pl.ds(low * capacity, (high - low) * capacity), slice(None))
-        return remote(
-            theirs.at[where],
-            arrived.at[where],
-            half_send.at[stage, turn_index],
-            half_recv.at[stage, turn_index],
-            partner,
-        )
-
-    def add_halves(turn_index, low, high):
-        for expert in range(local_count):
-            span = slice(low * capacity, high * capacity)
-            both = ours[turn_index, expert, span, :].astype(F32) + arrived[turn_index, expert, span, :].astype(F32)
-            ours[turn_index, expert, span, :] = both.astype(BF16)
-
-    def back_copy(turn_index, step):
-        return remote(
-            ours.at[turn_index, :, pl.ds(step * capacity, capacity), :],
-            returned.at[turn_index, step],
-            back_send.at[turn_index, step],
-            back_recv.at[turn_index, step],
-            at_ep(step),
-        )
-
-    back_copies = [[back_copy(q, step) for step in range(1, n)] for q in range(nz)]
-
-    core_copies[0].wait_recv()
+        pass_both(step)
     for step in range(1, n - 1):
-        core_copies[step].wait_recv()
-    experts_on(0, n - 1)
-    first_halves = [half_copy(0, q, 0, n - 1) for q in range(nz)]
-    for copy in first_halves:
-        copy.start()
-    out_copies[n - 2].wait_recv()
-    core_copies[n - 1].start()
-    for q in range(nz):
-        first_halves[q].wait_recv()
+        pass_share(step)
+    pass_out(n - 1)
+
+    def mixer_copy(x):
+        block = mixer_pair.at[xor(z, x, nz)]
+        return remote(block, mixer_in.at[x], mixer_send.at[x], mixer_recv.at[x], at_z(low_bit(x)))
+
+    mixer_copies = {x: mixer_copy(x) for x in order[:-1]}
+
+    def mixer_sum(x):
+        block = xor(z, x, nz)
+        total = mixer_pair[block].astype(F32)
+        for source in line_sources(x, nz):
+            mixer_copies[source].wait_recv()
+            total = total + mixer_in[source].astype(F32)
+        return total
+
+    def mixer_first():
+        for x in order[:-1]:
+            pair_sum(x)
+            if low_bit(x) == 1:
+                mixer_copies[x].start()
+
+    def mixer_next(bit):
+        for x in order[:-1]:
+            if low_bit(x) == bit:
+                mixer_pair[xor(z, x, nz)] = mixer_sum(x).astype(BF16)
+                mixer_copies[x].start()
+
+
+    mixer_first()
+    for step in range(1, n - 1):
+        wait_core(step)
+    for expert in range(local_count):
+        experts_on(1, n - 1, expert, expert + 1)
+        half_copies[1][expert].start()
+        if expert == 0:
+            pass_both(n - 1)
+            pass_share(n - 1)
+    wait_core(n - 1)
+    for expert in range(local_count):
+        experts_on(n - 1, n, expert, expert + 1)
+        half_copies[2][expert].start()
+        if expert == 0:
+            for stage in range(2):
+                for copy in half_copies[stage]:
+                    copy.wait_recv()
+            for q in range(EARLY):
+                add_halves(q, 0, n - 1)
+                for step in range(1, n - 1):
+                    back_copies[q][step - 1].start()
+    for q in range(EARLY, nz):
         add_halves(q, 0, n - 1)
-        if q < EARLY:
-            for step in range(1, n - 1):
-                back_copies[q][step - 1].start()
-    core_copies[n - 1].wait_recv()
-    experts_on(n - 1, n)
-    last_halves = [half_copy(1, q, n - 1, n) for q in range(nz)]
-    for copy in last_halves:
-        copy.start()
-    for q in range(nz):
-        last_halves[q].wait_recv()
-        add_halves(q, n - 1, n)
+    for copy in half_copies[2]:
+        copy.wait_recv()
+    def send_back(q):
         for step in range(1, n):
             if step == n - 1 or q >= EARLY:
                 back_copies[q][step - 1].start()
 
-    total = mixer_pair[z].astype(F32)
-    for step in range(1, nz):
-        mixer_copies[step - 1].wait_recv()
-        total = total + mixer_in[step].astype(F32)
-    mixer_ref[...] = total.astype(BF16)
-
-    line_copies = []
-    last = None
     for q in range(nz):
+        add_halves(q, n - 1, n)
+        if q < AHEAD:
+            send_back(q)
+
+    same = (iota((rows, rows), 0) == iota((rows, rows), 1)).astype(BF16)
+
+    @pl.loop(0, n)
+    def _(step):
+        group = xor(me, step, n)
+        upright = dot_nt(same, table[group].astype(BF16))
+        lane = iota((rows, batch), 1).astype(F32)
+        total = jnp.zeros((rows, batch), F32)
+        for expert in range(local_count):
+            spot = upright[:, expert : expert + 1] + float(expert * capacity)
+            gain = upright[:, local_count + expert : local_count + expert + 1]
+            total = total + jnp.where(lane == spot, gain, 0.0)
+        pick[step] = total.astype(BF16)
+
+
+    attend_line(0)
+    project_line(0)
+    pair_copies[0].start()
+
+    bit = 2
+    while bit < nz:
+        mixer_next(bit)
+        bit *= 2
+
+    def line_copy(q):
+        x = order[q]
+        return remote(combined.at[q], combined_in.at[x], line_send.at[x], line_recv.at[x], at_z(low_bit(x)))
+
+    line_copies = {order[q]: line_copy(q) for q in range(nz - 1)}
+    for q in range(nz):
+        x = order[q]
         own = ours[q, :, 0:capacity, :].reshape(batch, block_width)
-        last = dot(pick[0], own)
+        total = dot(pick[0], own)
         for step in range(1, n):
             back_copies[q][step - 1].wait_recv()
-            last = last + dot(pick[step], returned[q, step].reshape(batch, block_width))
-        if q < nz - 1:
-            combined[q] = last.astype(BF16)
-            step = nz - 1 - q
-            copy = remote(combined.at[q], combined_in.at[step], line_send.at[step], line_recv.at[step], at_z(step))
-            copy.start()
-            line_copies.append(copy)
-    for step in range(nz - 1, 0, -1):
-        line_copies[nz - 1 - step].wait_recv()
-        last = last + combined_in[step].astype(F32)
-    expert_out_ref[...] = last.astype(BF16)
-
-    sent = joint_copies + turned_copies + out_copies + core_copies + joint_cores + pair_copies
-    sent = sent + mixer_copies + first_halves + last_halves + line_copies
-    for copies in back_copies:
+            total = total + dot(pick[step], returned[q, step].reshape(batch, block_width))
+        if x == 0:
+            pair_sum(0)
+            mixer_ref[...] = mixer_sum(0).astype(BF16)
+        for source in line_sources(x, nz):
+            line_copies[source].wait_recv()
+            total = total + combined_in[source].astype(F32)
+        if x:
+            combined[q] = total.astype(BF16)
+            line_copies[x].start()
+            if q + AHEAD < nz:
+                send_back(q + AHEAD)
+        else:
+            expert_out_ref[...] = total.astype(BF16)
+
+    sent = joint_copies + joint_lines + joint_cores[0] + joint_cores[1] + turned_copies
+    sent = sent + out_copies + both_copies + share_copies + pair_copies
+    for copies in core_copies + back_copies + half_copies:
         sent = sent + copies
+    sent = sent + [mixer_copies[x] for x in order[:-1]] + [line_copies[x] for x in order[:-1]]
     for copy in sent:
         copy.wait_send()
 
@@ -581,7 +751,8 @@
         like(down_weight),
         pltpu.VMEM((n, 8, rows), F32),
         buffer(rows, half),
-        buffer(n - 1, local_count, capacity, half),
+        buffer(n - 1, local_count, capacity, half * SHARED_EIGHTHS // 8),
+        buffer(n - 1, local_count, capacity, half - 2 * (half * SHARED_EIGHTHS // 8)),
         buffer(2, local_count, n * capacity, half),
         buffer(n, rows, batch),
         buffer(n, turn, rows),
@@ -600,7 +771,8 @@
         buffer(nz, rows, block_width),
         dma((12,)),
     ]
-    for shape in ((n,), (n,), (n,), (n,), (n,), (nz,), (nz,), (2, nz), (nz, n), (nz,)):
+    line = [(n,), (n,), (2, n), (n,), (n,), (n,), (n,), (3, n), (nz,), (nz,), (3, local_count), (nz, n), (nz,)]
+    for shape in line:
         scratch += [dma(shape), dma(shape)]
 
     vmem = pl.BlockSpec(memory_space=pltpu.VMEM)

time: 101 us -> 91.7 us (0.908)
  Pallas kernels: 97 us -> 87.4 us
    pallas_call x1, Pallas kernels: 97 us -> 87.4 us  [local(): pl.pallas_call(functools.partial(kernel, dims), in_specs=[vmem] * len(sma...]
where the time goes in v2:
time: 91.7 us; the launch traced here: 91.4 us
  Pallas kernels  87.4 us (95%)
  local copies, waits for them, and re-layouts  3.34 us (4%)
    pallas_call x1, Pallas kernels, local(): pl.pallas_call(functools.partial(kernel, dims), in_specs=[vmem] * len(sma...  87.4 us
    unnamed x2, local copies, waits for them, and re-layouts  3.34 us

profile of v2, /device:TPU:0, one launch (start us, length us, event | category | flops | bytes accessed | tf_op | source)
XLA Modules:
  0.0 91.4 jit_solution(6165029719779351443)
XLA Ops:
  0.6 87.4 %whole.1 = (bf16[64,2048]{1,0:T(8,128)(2,1)}, bf16[512,256]{1,0:T(8,128)(2,1)}) custom-call(s32[2,512]{1,0:T(2,128)} %bitcast.8, f32[2,512]{1,0:T(2,128)} %bitcast.9, bf16[32,512]{1,0:T(8,128)(2,1)} %bitcast.6, f32[16,1]{1,0:T(8,128)} %constant.4.clone.freq_col_ref, f32[1,128]{1,0:T(1,128)} %constant.5.clone.freq_row_ref, f32[1,1024]{1,0:T(1,128)} %bitcast.10, ...), custom_call_target="tpu_custom_call" | custom-call | tf_op jit(solution)/shard_map/whole/pallas_call | solution.py:780
  88.1 1.7 %copy.23 = bf16[64,2048]{1,0:T(8,128)(2,1)} copy(bf16[64,2048]{1,0:T(8,128)(2,1)} %get-tuple-element.4) | data formatting | bytes 524288
  89.8 1.7 %copy.24 = bf16[512,256]{1,0:T(8,128)(2,1)} copy(bf16[512,256]{1,0:T(8,128)(2,1)} %get-tuple-element.5) | data formatting | bytes 524288

commit v3 on v2

--- a/solution.py
+++ b/solution.py
@@ -532,18 +532,19 @@
         both = partial[2 * block + c].astype(F32) + mixer_pair[block].astype(F32)
         mixer_pair[block] = both.astype(BF16)
 
-    for x in order[:-1]:
+    for i, x in enumerate(order[:-1]):
         attend_line(x)
+        if i == nz // 2 - 1:
+            pass_out(n - 1)
+    for step in range(1, n - 1):
+        pass_both(step)
     loads[8].wait()
     for x in order[:-1]:
         project_line(x)
         pair_copies[x].start()
 
     for step in range(1, n - 1):
-        pass_both(step)
-    for step in range(1, n - 1):
         pass_share(step)
-    pass_out(n - 1)
 
     def mixer_copy(x):
         block = mixer_pair.at[xor(z, x, nz)]

time: 91.7 us -> 93.3 us (1.017)
  Pallas kernels: 87.4 us -> 89.1 us
    pallas_call x1, Pallas kernels: 87.4 us -> 89.1 us  [local(): pl.pallas_call(functools.partial(kernel, dims), in_specs=[vmem] * len(sma...]
where the time goes in v3:
time: 93.3 us; the launch traced here: 93.1 us
  Pallas kernels  89.1 us (95%)
  local copies, waits for them, and re-layouts  3.34 us (4%)
    pallas_call x1, Pallas kernels, local(): pl.pallas_call(functools.partial(kernel, dims), in_specs=[vmem] * len(sma...  89.1 us
    unnamed x2, local copies, waits for them, and re-layouts  3.34 us

profile of v3, /device:TPU:0, one launch (start us, length us, event | category | flops | bytes accessed | tf_op | source)
XLA Modules:
  0.0 93.1 jit_solution(8581318448737193066)
XLA Ops:
  0.6 89.1 %whole.1 = (bf16[64,2048]{1,0:T(8,128)(2,1)}, bf16[512,256]{1,0:T(8,128)(2,1)}) custom-call(s32[2,512]{1,0:T(2,128)} %bitcast.8, f32[2,512]{1,0:T(2,128)} %bitcast.9, bf16[32,512]{1,0:T(8,128)(2,1)} %bitcast.6, f32[16,1]{1,0:T(8,128)} %constant.4.clone.freq_col_ref, f32[1,128]{1,0:T(1,128)} %constant.5.clone.freq_row_ref, f32[1,1024]{1,0:T(1,128)} %bitcast.10, ...), custom_call_target="tpu_custom_call" | custom-call | tf_op jit(solution)/shard_map/whole/pallas_call | solution.py:781
  89.8 1.7 %copy.23 = bf16[64,2048]{1,0:T(8,128)(2,1)} copy(bf16[64,2048]{1,0:T(8,128)(2,1)} %get-tuple-element.4) | data formatting | bytes 524288
  91.4 1.7 %copy.24 = bf16[512,256]{1,0:T(8,128)(2,1)} copy(bf16[512,256]{1,0:T(8,128)(2,1)} %get-tuple-element.5) | data formatting | bytes 524288
